TPU v7x, 32 devices: a whole 2x2x4 slice. The times are simulated.
32 devices in a mesh: sp: 8 (over z, x), tp: 4 (over y, core).
Axes of the slice: x: 2, y: 2, z: 4, core: 2. Of those that a mesh axis runs over, the one named last changes fastest.
Arguments:
- glu_value: bfloat16 [1536, 1024], P('sp', 'tp'), may hold values from -6 to 6
- glu_gate: bfloat16 [1536, 1024], P('sp', 'tp'), may hold values from -6 to 6
- doc_ids: int32 [1536], P('sp'), may hold values from 0 to 3, never falling along the last dimension, each value on 1 to 768 neighbouring positions
- conv_kernel: bfloat16 [31, 1024], P(None, 'tp')
- conv_gain: float32 [1024], P('tp'), may hold values from 0.1 to 1.9
- out_weight: bfloat16 [1024, 2048], P('tp'), may hold values from -0.1875 to 0.1875
- residual: bfloat16 [1536, 2048], P('sp'), may hold values from -6 to 6
- mix_gain: float32 [2048], replicated, may hold values from 0.1 to 1.9
- routes: int32 [1536, 2], P('sp'), may hold values from 0 to 7, all different within a row; in each aligned block of 192 rows (0 to 191, 192 to 383, ...) at most 96 rows name the same one
- route_weights: float32 [1536, 2], P('sp'), may hold values from 0.2 to 1
- expert_gate: bfloat16 [8, 2048, 5120], P('sp', None, 'tp'), may hold values from -0.125 to 0.125
- expert_up: bfloat16 [8, 2048, 5120], P('sp', None, 'tp'), may hold values from -0.125 to 0.125
- expert_down: bfloat16 [8, 5120, 2048], P('sp', 'tp')
- final_gain: float32 [2048], P('tp'), may hold values from 0.1 to 1.9
Outputs:
- block_out: bfloat16 [1536, 2048], P('sp', 'tp')
Inputs may be any that keep to these rules, and one draw needn't show every extreme that they name: `routes`: each row names two different experts. In each aligned block of 192 rows no expert is named by more than 96 rows, and in every draw some block has an expert named by exactly 96 rows. `doc_ids`: document numbers never fall along the sequence.
All inputs are finite; a program needn't handle non-finite values.
Results may differ from a plain program's by a relative error of at most 0.022.
Values may be sent and summed in bfloat16 or wider, within the bound.
A program may use at most 64 MiB of HBM per device.

v0:
```python
import functools

import jax
import jax.numpy as jnp
from jax import lax
from jax.experimental import pallas as pl
from jax.experimental.pallas import tpu as pltpu
from jax.sharding import PartitionSpec as P

residual_alpha = 1.41421356
norm_eps = 1e-05


def from_behind(value, axis, by):
    peers = lax.axis_size(axis)
    pairs = [(i, i + by) for i in range(peers) if 0 <= i + by < peers]
    return lax.ppermute(value, axis, pairs)


def scaled_norm(pre_norm, gain):
    row_mean = jnp.mean(pre_norm, -1, keepdims=True)
    row_var = jnp.mean(pre_norm * pre_norm, -1, keepdims=True) - row_mean * row_mean
    return (pre_norm - row_mean) * lax.rsqrt(row_var + norm_eps) * gain


def local_plain(
    glu_value,
    glu_gate,
    doc_ids,
    conv_kernel,
    conv_gain,
    out_weight,
    residual,
    mix_gain,
    routes,
    route_weights,
    expert_gate,
    expert_up,
    expert_down,
    final_gain,
):
    tok_rows = glu_value.shape[0]
    rim_len = conv_kernel.shape[0] - 1
    channels = glu_value.shape[1] * lax.axis_size("tp")
    gated_rows = (
        glu_value.astype(jnp.float32) * jax.nn.sigmoid(glu_gate.astype(jnp.float32))
    ).astype(jnp.bfloat16)
    rim_rows, rim_ids = from_behind(
        (gated_rows[tok_rows - rim_len :], doc_ids[tok_rows - rim_len :]), "sp", 1
    )
    extended = jnp.concatenate([rim_rows, gated_rows], 0).astype(jnp.float32)
    ext_ids = jnp.concatenate([rim_ids, doc_ids], 0)
    kernel = conv_kernel.astype(jnp.float32)
    filtered = jnp.zeros(gated_rows.shape, jnp.float32)
    for shift_by in range(rim_len + 1):
        begin_at = rim_len - shift_by
        same_doc = (ext_ids[begin_at : begin_at + tok_rows] == doc_ids)[:, None]
        filtered = (
            filtered
            + jnp.where(same_doc, extended[begin_at : begin_at + tok_rows], 0.0) * kernel[shift_by]
        )
    row_sum, row_square = lax.psum((jnp.sum(filtered, 1), jnp.sum(filtered * filtered, 1)), "tp")
    row_mean = row_sum[:, None] / channels
    row_var = row_square[:, None] / channels - row_mean * row_mean
    conv_out = jax.nn.silu(
        (filtered - row_mean) * lax.rsqrt(row_var + norm_eps) * conv_gain
    ).astype(jnp.bfloat16)
    mix_total = lax.psum(
        jnp.dot(conv_out, out_weight, preferred_element_type=jnp.float32).astype(jnp.bfloat16), "tp"
    ).astype(jnp.float32)
    mixed_rows = scaled_norm(
        residual_alpha * residual.astype(jnp.float32) + mix_total, mix_gain
    ).astype(jnp.bfloat16)
    experts = expert_gate.shape[0] * lax.axis_size("sp")
    capacity = 4 * tok_rows // experts
    chosen = routes.reshape(-1)
    member = (chosen[:, None] == jnp.arange(experts, dtype=jnp.int32)[None, :]).astype(jnp.int32)
    earlier = jnp.cumsum(member, 0) - member
    slot_index = chosen * capacity + jnp.sum(earlier * member, 1)
    dispatch_table = jnp.any(
        jnp.arange(experts * capacity, dtype=jnp.int32)[:, None, None]
        == slot_index.reshape(tok_rows, 2)[None],
        -1,
    ).astype(jnp.bfloat16)
    feat_block = mixed_rows.shape[1] // lax.axis_size("tp")
    offset = lax.axis_index("tp") * feat_block
    w_gate = expert_gate[0]
    w_up = expert_up[0]
    w_down = expert_down[0]
    row_slice = lax.dynamic_slice_in_dim(mixed_rows, offset, feat_block, 1)
    outgoing = (
        jnp.dot(dispatch_table, row_slice, preferred_element_type=jnp.float32)
        .astype(jnp.bfloat16)
        .reshape(experts, capacity, feat_block)
    )
    arrived = lax.all_to_all(outgoing, "sp", split_axis=0, concat_axis=0, tiled=True)
    sources, slot_count, part_width = arrived.shape
    flat_rows = arrived.reshape(sources * slot_count, part_width)
    col_piece = lax.all_gather(flat_rows, "tp", axis=1, tiled=True)
    gate_proj = jnp.dot(col_piece, w_gate, preferred_element_type=jnp.float32)
    up_proj = jnp.dot(col_piece, w_up, preferred_element_type=jnp.float32)
    hidden = (jax.nn.silu(gate_proj) * up_proj).astype(jnp.bfloat16)
    partial_value = jnp.dot(hidden, w_down, preferred_element_type=jnp.float32).reshape(
        sources, slot_count, -1
    )
    summed = lax.psum_scatter(
        partial_value.astype(jnp.bfloat16), "tp", scatter_dimension=2, tiled=True
    )
    returned = lax.all_to_all(summed, "sp", split_axis=0, concat_axis=0, tiled=True)
    flat_back = returned.reshape(experts * capacity, feat_block)
    picked = flat_back[slot_index].astype(jnp.float32).reshape(tok_rows, 2, feat_block)
    moe_sum = jnp.sum(route_weights[:, :, None] * picked, 1)
    own_cols = lax.dynamic_slice_in_dim(mixed_rows, offset, feat_block, 1).astype(jnp.float32)
    pre_norm = residual_alpha * own_cols + moe_sum
    fin_sum, fin_square = lax.psum((jnp.sum(pre_norm, 1), jnp.sum(pre_norm * pre_norm, 1)), "tp")
    features = feat_block * lax.axis_size("tp")
    fin_mean = fin_sum[:, None] / features
    fin_var = fin_square[:, None] / features - fin_mean * fin_mean
    return ((pre_norm - fin_mean) * lax.rsqrt(fin_var + norm_eps) * final_gain).astype(jnp.bfloat16)


HALO = 32
GROUPS = 2
TILE = 256
F32 = jnp.float32
BF16 = jnp.bfloat16


def block_kernel(
    sp_n,
    tp_n,
    capacity,
    taps,
    glu_value,
    glu_gate,
    ids,
    conv_kernel,
    conv_gain,
    out_weight_hbm,
    residual_hbm,
    mix_gain,
    routes_col,
    routes_row,
    route_weights,
    gate_hbm,
    up_hbm,
    down_hbm,
    final_gain,
    out,
    w_out,
    resid,
    w_gate,
    w_up,
    w_down,
    halo_v,
    halo_g,
    halo_i,
    ext,
    ext_ids,
    fil,
    stat_out,
    stat_in,
    mix_pp,
    mix_a,
    mix_s,
    mix_b,
    mixed,
    outbox,
    rows_in,
    hidden,
    part_pp,
    part_a,
    part_s,
    part_b,
    part_own,
    back_out,
    back_in,
    load_sem,
    halo_sem,
    stat_send,
    stat_recv,
    mix_send,
    mix_recv,
    disp_send,
    disp_recv,
    ag_send,
    ag_recv,
    part_send,
    part_recv,
    cross_send,
    cross_recv,
    back_send,
    back_recv,
):
    tok = glu_value.shape[0]
    chan = glu_value.shape[1]
    feat = final_gain.shape[1]
    ff = hidden.shape[2]
    y_n = tp_n // 2
    sp = lax.axis_index("sp")
    tp = lax.axis_index("tp")
    y = tp // 2
    core = tp % 2
    partner = y * 2 + (1 - core)
    group_d = sp_n // GROUPS
    group_rows = group_d * capacity
    pending = []

    def y_at(k):
        return lax.rem(y + k, y_n)

    def feat_cols(block):
        return pl.ds(pl.multiple_of(block * feat, feat), feat)

    def remote(src, dst, send, recv, axis, to):
        return pltpu.make_async_remote_copy(
            src_ref=src,
            dst_ref=dst,
            send_sem=send,
            recv_sem=recv,
            device_id={axis: to},
            device_id_type=pl.DeviceIdType.MESH,
        )

    def send(*args):
        copy = remote(*args)
        copy.start()
        pending.append(copy)

    def arrived(dst, recv, send_sem, axis, to):
        remote(dst, dst, send_sem, recv, axis, to).wait_recv()

    loads = []
    for i, (src, dst) in enumerate(
        (
            (out_weight_hbm, w_out),
            (residual_hbm.at[:, feat_cols(tp)], resid),
            (gate_hbm.at[0], w_gate),
            (up_hbm.at[0], w_up),
            (down_hbm.at[0], w_down),
        )
    ):
        copy = pltpu.make_async_copy(src, dst, load_sem.at[i])
        copy.start()
        loads.append(copy)

    barrier = pltpu.get_barrier_semaphore()
    for k in range(1, sp_n):
        pl.semaphore_signal(
            barrier, inc=1, device_id={"sp": lax.rem(sp + k, sp_n)},
            device_id_type=pl.DeviceIdType.MESH,
        )
    for k in range(1, tp_n):
        pl.semaphore_signal(
            barrier, inc=1, device_id={"tp": lax.rem(tp + k, tp_n)},
            device_id_type=pl.DeviceIdType.MESH,
        )
    pl.semaphore_wait(barrier, sp_n + tp_n - 2)

    right = lax.rem(sp + 1, sp_n)
    rim = pl.ds(tok - HALO, HALO)
    halo = (
        (glu_value, halo_v),
        (glu_gate, halo_g),
        (ids, halo_i),
    )
    for i, (src, dst) in enumerate(halo):
        send(src.at[rim], dst, halo_sem.at[0, i], halo_sem.at[1, i], "sp", right)

    def gated(value, gate):
        value = value.astype(F32)
        return (value * jax.nn.sigmoid(gate.astype(F32))).astype(BF16).astype(F32)

    ext[HALO:, :] = gated(glu_value[...], glu_gate[...])
    ext_ids[HALO:, :] = ids[...]

    experts = sp_n
    lower = (
        lax.broadcasted_iota(jnp.int32, (tok, tok), 1)
        < lax.broadcasted_iota(jnp.int32, (tok, tok), 0)
    )
    upper = (
        lax.broadcasted_iota(jnp.int32, (tok, tok), 0)
        < lax.broadcasted_iota(jnp.int32, (tok, tok), 1)
    )
    lanes = 128
    e_lane = lax.broadcasted_iota(jnp.int32, (tok, lanes), 1)
    rel_col = lax.rem(routes_col[...] - sp + experts, experts)
    m0 = (rel_col[:, 0:1] == e_lane).astype(F32)
    m1 = (rel_col[:, 1:2] == e_lane).astype(F32)
    rank = jnp.dot(lower.astype(F32).astype(BF16), (m0 + m1).astype(BF16), preferred_element_type=F32)
    place = rank + (e_lane * capacity).astype(F32)
    slot_col0 = jnp.sum(m0 * place, 1, keepdims=True).astype(jnp.int32)
    slot_col1 = jnp.sum(m1 * place, 1, keepdims=True).astype(jnp.int32)
    e_sub = lax.broadcasted_iota(jnp.int32, (lanes, tok), 0)
    rel_row = lax.rem(routes_row[...] - sp + experts, experts)
    n0 = (rel_row[0:1, :] == e_sub).astype(F32)
    n1 = (rel_row[1:2, :] == e_sub).astype(F32)
    rank_r = jnp.dot((n0 + n1).astype(BF16), upper.astype(F32).astype(BF16), preferred_element_type=F32)
    place_r = rank_r + (e_sub * capacity).astype(F32)
    slot_row0 = jnp.sum(n0 * place_r, 0, keepdims=True).astype(jnp.int32)
    slot_row1 = jnp.sum(n1 * place_r, 0, keepdims=True).astype(jnp.int32)

    for i, (_, dst) in enumerate(halo):
        arrived(dst, halo_sem.at[1, i], halo_sem.at[0, i], "sp", right)
    first = jnp.where(sp == 0, 1, 0)
    ext[:HALO, :] = gated(halo_v[...], halo_g[...])
    ext_ids[:HALO, :] = halo_i[...] * (1 - first) - first

    kern = conv_kernel[...].astype(F32)
    step = 32
    lane_blocks = chan // lanes
    for at in range(0, tok, step):
        own = ids[at : at + step, :]
        acc = [jnp.zeros((step, lanes), F32) for _ in range(lane_blocks)]
        for lag in range(taps):
            begin = HALO + at - lag
            same = ext_ids[begin : begin + step, :] == own
            for b in range(lane_blocks):
                part = ext[begin : begin + step, b * lanes : (b + 1) * lanes]
                acc[b] = acc[b] + jnp.where(same, part, 0.0) * kern[lag : lag + 1, b * lanes : (b + 1) * lanes]
        for b in range(lane_blocks):
            fil[at : at + step, b * lanes : (b + 1) * lanes] = acc[b]

    def stats(i, value, width):
        row_sum = jnp.sum(value, 1, keepdims=True)
        row_square = jnp.sum(value * value, 1, keepdims=True)
        packed = jnp.where(e_lane == 0, row_sum, jnp.where(e_lane == 1, row_square, 0.0))
        wide = stat_out.shape[2]
        packed = jnp.concatenate([packed, jnp.zeros((wide - tok, lanes), F32)], 0)
        stat_out[i] = packed.T[:8]
        for k in range(1, tp_n):
            send(
                stat_out.at[i], stat_in.at[i, k], stat_send.at[i, k], stat_recv.at[i, k],
                "tp", lax.rem(tp + k, tp_n),
            )
        total = stat_out[i]
        for k in range(1, tp_n):
            arrived(stat_in.at[i, k], stat_recv.at[i, k], stat_send.at[i, k], "tp", partner)
            total = total + stat_in[i, k]
        total = jnp.concatenate([total, jnp.zeros((lanes - 8, wide), F32)], 0).T[:tok]
        mean = total[:, 0:1] / width
        var = total[:, 1:2] / width - mean * mean
        return mean, lax.rsqrt(var + norm_eps)

    filtered = fil[...]
    mean, scale = stats(0, filtered, chan * tp_n)
    normed = (filtered - mean) * scale * conv_gain[...]
    conv_out = (normed * jax.nn.sigmoid(normed)).astype(BF16)

    loads[0].wait()
    order = list(range(1, y_n)) + [0]
    for k in order:
        cols = feat_cols(2 * y_at(k) + 1 - core)
        mix_pp[k] = jnp.dot(conv_out, w_out[:, cols], preferred_element_type=F32).astype(BF16)
        send(mix_pp.at[k], mix_a.at[k], mix_send.at[0, k], mix_recv.at[0, k], "tp", partner)
    own_mix = None
    for k in order:
        cols = feat_cols(2 * y_at(k) + core)
        value = jnp.dot(conv_out, w_out[:, cols], preferred_element_type=F32)
        arrived(mix_a.at[k], mix_recv.at[0, k], mix_send.at[0, k], "tp", partner)
        value = value + mix_a[k].astype(F32)
        if k:
            mix_s[k] = value.astype(BF16)
            send(
                mix_s.at[k], mix_b.at[k], mix_send.at[1, k], mix_recv.at[1, k],
                "tp", 2 * y_at(k) + core,
            )
        else:
            own_mix = value
    loads[1].wait()
    pre = own_mix + residual_alpha * resid[...].astype(F32)
    for k in range(1, y_n):
        arrived(mix_b.at[k], mix_recv.at[1, k], mix_send.at[1, k], "tp", partner)
        pre = pre + mix_b[k].astype(F32)
    mean, scale = stats(1, pre, feat * tp_n)
    mixed[...] = ((pre - mean) * scale * mix_gain[:, feat_cols(tp)]).astype(BF16)

    def spread(d):
        block = rows_in.at[tp, d]
        send(block, block, ag_send.at[0, d], ag_recv.at[0, d], "tp", partner)
        for k in range(1, y_n):
            send(
                block, block, ag_send.at[k, d], ag_recv.at[k, d],
                "tp", 2 * y_at(k) + core,
            )

    def pass_on(d):
        for k in range(1, y_n):
            block = rows_in.at[2 * y_at(y_n - k) + core, d]
            arrived(block, ag_recv.at[k, d], ag_send.at[k, d], "tp", partner)
            send(
                block, block, ag_send.at[y_n - 1 + k, d], ag_recv.at[y_n - 1 + k, d],
                "tp", partner,
            )

    def gathered(d):
        block = rows_in.at[partner, d]
        arrived(block, ag_recv.at[0, d], ag_send.at[0, d], "tp", partner)
        for k in range(1, y_n):
            block = rows_in.at[2 * y_at(y_n - k) + 1 - core, d]
            arrived(block, ag_recv.at[y_n - 1 + k, d], ag_send.at[y_n - 1 + k, d], "tp", partner)

    for d in list(range(1, sp_n)) + [0]:
        s_at = lax.broadcasted_iota(jnp.int32, (capacity, tok), 0) + d * capacity
        table = jnp.logical_or(s_at == slot_row0, s_at == slot_row1).astype(F32).astype(BF16)
        block = jnp.dot(table, mixed[...], preferred_element_type=F32).astype(BF16)
        if d:
            outbox[d] = block
            send(
                outbox.at[d], rows_in.at[tp, d], disp_send.at[d], disp_recv.at[d],
                "sp", lax.rem(sp + d, sp_n),
            )
        else:
            rows_in[tp, 0] = block

    def landed(d):
        if d:
            arrived(rows_in.at[tp, d], disp_recv.at[d], disp_send.at[d], "sp", right)
        spread(d)

    def gate_up(g, lo, hi):
        @pl.loop(lo, hi)
        def _(n):
            cols = pl.ds(pl.multiple_of(n * TILE, TILE), TILE)
            rows = [
                rows_in[j, g * group_d : (g + 1) * group_d].reshape(group_rows, feat)
                for j in range(tp_n)
            ]
            x = jnp.concatenate(rows, 1)
            gate = jnp.dot(x, w_gate[:, cols], preferred_element_type=F32)
            up = jnp.dot(x, w_up[:, cols], preferred_element_type=F32)
            hidden[g, :, cols] = (gate * jax.nn.sigmoid(gate) * up).astype(BF16)

    def down_tile(g, block, t):
        cols = pl.ds(pl.multiple_of(block * feat + t * TILE, TILE), TILE)
        return jnp.dot(hidden[g], w_down[:, cols], preferred_element_type=F32)

    def down(g, between=lambda: None):
        for k in order:
            block = 2 * y_at(k) + 1 - core

            @pl.loop(0, feat // TILE)
            def _(t):
                cols = pl.ds(pl.multiple_of(t * TILE, TILE), TILE)
                part_pp[g, k, :, cols] = down_tile(g, block, t).astype(BF16)

            send(
                part_pp.at[g, k], part_a.at[g, k], part_send.at[g, k], part_recv.at[g, k],
                "tp", partner,
            )
        between()
        for k in order:
            block = 2 * y_at(k) + core
            arrived(part_a.at[g, k], part_recv.at[g, k], part_send.at[g, k], "tp", partner)

            @pl.loop(0, feat // TILE)
            def _(t):
                cols = pl.ds(pl.multiple_of(t * TILE, TILE), TILE)
                value = down_tile(g, block, t) + part_a[g, k, :, cols].astype(F32)
                if k:
                    part_s[g, k, :, cols] = value.astype(BF16)
                else:
                    part_own[g, :, cols] = value

            for i in range(group_d if k else 0):
                rows = pl.ds(i * capacity, capacity)
                send(
                    part_s.at[g, k, rows], part_b.at[g, k, rows],
                    cross_send.at[g, k, i], cross_recv.at[g, k, i],
                    "tp", 2 * y_at(k) + core,
                )

    def finish(g, i):
        d = g * group_d + i
        rows = pl.ds(i * capacity, capacity)
        value = part_own[g, rows, :]
        for k in range(1, y_n):
            arrived(
                part_b.at[g, k, rows], cross_recv.at[g, k, i], cross_send.at[g, k, i],
                "tp", partner,
            )
            value = value + part_b[g, k, rows, :].astype(F32)
        if d:
            back_out[d] = value.astype(BF16)
            send(
                back_out.at[d], back_in.at[d], back_send.at[d], back_recv.at[d],
                "sp", lax.rem(sp - d + sp_n, sp_n),
            )
        else:
            back_in[0] = value.astype(BF16)

    for d in range(group_d):
        landed(d)
        if d:
            pass_on(d - 1)
    pass_on(group_d - 1)
    for d in range(group_d):
        gathered(d)
    loads[2].wait()
    loads[3].wait()
    tiles = ff // TILE
    for n in range(tiles):
        gate_up(0, n, n + 1)
        if n < group_d:
            landed(group_d + n)
        if 1 <= n <= group_d:
            pass_on(group_d + n - 1)
    for i in range(min(tiles, group_d), group_d):
        landed(group_d + i)
    for i in range(min(max(tiles - 1, 0), group_d), group_d):
        pass_on(group_d + i)
    loads[4].wait()
    down(0)
    for d in range(group_d, sp_n):
        gathered(d)
    half = tiles // 2
    gate_up(1, 0, half)
    finish(0, 0)
    gate_up(1, half, tiles)
    for i in range(1, group_d // 2):
        finish(0, i)
    down(1, lambda: [finish(0, i) for i in range(max(1, group_d // 2), group_d)])
    for i in range(group_d):
        finish(1, i)

    for d in range(1, sp_n):
        arrived(back_in.at[d], back_recv.at[d], back_send.at[d], "sp", right)
    slots = sp_n * capacity
    returned = back_in[...].reshape(slots, feat)
    s_lane = lax.broadcasted_iota(jnp.int32, (tok, slots), 1)
    pick0 = jnp.dot((s_lane == slot_col0).astype(F32).astype(BF16), returned, preferred_element_type=F32)
    pick1 = jnp.dot((s_lane == slot_col1).astype(F32).astype(BF16), returned, preferred_element_type=F32)
    moe = route_weights[:, 0:1] * pick0 + route_weights[:, 1:2] * pick1
    pre = residual_alpha * mixed[...].astype(F32) + moe
    mean, scale = stats(2, pre, feat * tp_n)
    out[...] = ((pre - mean) * scale * final_gain[...]).astype(BF16)
    for copy in pending:
        copy.wait_send()


def local_kernel(
    glu_value,
    glu_gate,
    doc_ids,
    conv_kernel,
    conv_gain,
    out_weight,
    residual,
    mix_gain,
    routes,
    route_weights,
    expert_gate,
    expert_up,
    expert_down,
    final_gain,
):
    sp_n, tp_n = lax.axis_size("sp"), lax.axis_size("tp")
    tok, chan = glu_value.shape
    feat = final_gain.shape[0]
    width, ff = expert_gate.shape[1:]
    capacity = 4 * tok // sp_n
    y_n = tp_n // 2
    rows = sp_n // GROUPS * capacity
    wide = -(-tok // 128) * 128
    vmem = pl.BlockSpec(memory_space=pltpu.VMEM)
    hbm = pl.BlockSpec(memory_space=pl.ANY)
    dma = pltpu.SemaphoreType.DMA
    scratch = [
        pltpu.VMEM((chan, width), BF16),
        pltpu.VMEM((tok, feat), BF16),
        pltpu.VMEM((width, ff), BF16),
        pltpu.VMEM((width, ff), BF16),
        pltpu.VMEM((ff, width), BF16),
        pltpu.VMEM((HALO, chan), BF16),
        pltpu.VMEM((HALO, chan), BF16),
        pltpu.VMEM((HALO, 128), jnp.int32),
        pltpu.VMEM((HALO + tok, chan), F32),
        pltpu.VMEM((HALO + tok, 128), jnp.int32),
        pltpu.VMEM((tok, chan), F32),
        pltpu.VMEM((3, 8, wide), F32),
        pltpu.VMEM((3, tp_n, 8, wide), F32),
        pltpu.VMEM((y_n, tok, feat), BF16),
        pltpu.VMEM((y_n, tok, feat), BF16),
        pltpu.VMEM((y_n, tok, feat), BF16),
        pltpu.VMEM((y_n, tok, feat), BF16),
        pltpu.VMEM((tok, feat), BF16),
        pltpu.VMEM((sp_n, capacity, feat), BF16),
        pltpu.VMEM((tp_n, sp_n, capacity, feat), BF16),
        pltpu.VMEM((GROUPS, rows, ff), BF16),
        pltpu.VMEM((GROUPS, y_n, rows, feat), BF16),
        pltpu.VMEM((GROUPS, y_n, rows, feat), BF16),
        pltpu.VMEM((GROUPS, y_n, rows, feat), BF16),
        pltpu.VMEM((GROUPS, y_n, rows, feat), BF16),
        pltpu.VMEM((GROUPS, rows, feat), F32),
        pltpu.VMEM((sp_n, capacity, feat), BF16),
        pltpu.VMEM((sp_n, capacity, feat), BF16),
        dma((5,)),
        dma((2, 3)),
        dma((3, tp_n)),
        dma((3, tp_n)),
        dma((2, y_n)),
        dma((2, y_n)),
        dma((sp_n,)),
        dma((sp_n,)),
        dma((2 * y_n - 1, sp_n)),
        dma((2 * y_n - 1, sp_n)),
        dma((GROUPS, y_n)),
        dma((GROUPS, y_n)),
        dma((GROUPS, y_n, sp_n // GROUPS)),
        dma((GROUPS, y_n, sp_n // GROUPS)),
        dma((sp_n,)),
        dma((sp_n,)),
    ]
    return pl.pallas_call(
        functools.partial(block_kernel, sp_n, tp_n, capacity, conv_kernel.shape[0]),
        out_shape=jax.ShapeDtypeStruct((tok, feat), BF16),
        in_specs=[vmem] * 5 + [hbm] * 2 + [vmem] * 4 + [hbm] * 3 + [vmem],
        out_specs=vmem,
        scratch_shapes=scratch,
        compiler_params=pltpu.CompilerParams(
            collective_id=0, has_side_effects=True, vmem_limit_bytes=60 * 1024 * 1024
        ),
    )(
        glu_value,
        glu_gate,
        jnp.broadcast_to(doc_ids[:, None], (tok, 128)),
        conv_kernel,
        conv_gain[None, :],
        out_weight,
        residual,
        mix_gain[None, :],
        routes,
        routes.T,
        route_weights,
        expert_gate,
        expert_up,
        expert_down,
        final_gain[None, :],
    )


def local(*args):
    sp_n, tp_n = lax.axis_size("sp"), lax.axis_size("tp")
    tok, chan = args[0].shape
    ff = args[10].shape[2]
    feat = args[13].shape[0]
    aligned = (
        chan % 128 == 0
        and feat % TILE == 0
        and ff % TILE == 0
        and (4 * tok // sp_n) % 32 == 0
        and tok % HALO == 0
        and args[3].shape[0] <= HALO
        and tp_n % 2 == 0
        and tp_n > 2
        and sp_n % GROUPS == 0
        and sp_n > GROUPS
        and sp_n <= 128
        and args[10].shape[0] == 1
    )
    return (local_kernel if aligned else local_plain)(*args)


def solution(mesh):
    return jax.shard_map(
        local,
        mesh=mesh,
        in_specs=(
            P("sp", "tp"),
            P("sp", "tp"),
            P("sp"),
            P(None, "tp"),
            P("tp"),
            P("tp", None),
            P("sp", None),
            P(),
            P("sp", None),
            P("sp", None),
            P("sp", None, "tp"),
            P("sp", None, "tp"),
            P("sp", "tp", None),
            P("tp"),
        ),
        out_specs=P("sp", "tp"),
        check_vma=False,
    )
```

profile of v0, /device:TPU:0, one launch (start us, length us, event | category | flops | bytes accessed | tf_op | source)
XLA Modules:
  0.0 101.4 jit_solution(12910758830855206433)
XLA Ops:
  0.0 1.4 %broadcast_in_dim.15.ids = s32[192,128]{1,0:T(8,128)} broadcast(s32[192]{0:T(256)} %param.16), dimensions={0} | broadcast | bytes 99072 | tf_op jit(solution)/shard_map/broadcast_in_dim | solution.py:627
  1.4 1.5 %copy.16.route_weights = f32[192,2]{1,0:T(8,128)} copy(f32[192,2]{0,1:T(2,128)} %param.23) | data formatting | bytes 3072 | tf_op args[9]
  2.9 1.4 %copy.15.routes_col = s32[192,2]{1,0:T(8,128)} copy(s32[192,2]{0,1:T(2,128)} %param.22) | data formatting | bytes 3072 | tf_op args[8]
  4.3 95.5 %shard_map.136 = bf16[192,512]{1,0:T(8,128)(2,1)} custom-call(bf16[192,256]{1,0:T(8,128)(2,1)} %glu_value.1, bf16[192,256]{1,0:T(8,128)(2,1)} %glu_gate.1, s32[192,128]{1,0:T(8,128)} %broadcast_in_dim.15.ids, bf16[31,256]{1,0:T(8,128)(2,1)} %conv_kernel.1, f32[1,256]{1,0:T(1,128)} %bitcast.7, bf16[256,2048]{1,0:T(8,128)(2,1)} %out_weight_hbm.1, ...), custom_call_target="tpu_custom_call" | custom-call | tf_op jit(solution)/shard_map/pallas_call | solution.py:615
  99.8 1.6 %copy.18 = bf16[192,512]{1,0:T(8,128)(2,1)} copy(bf16[192,512]{1,0:T(8,128)(2,1)} %shard_map.136) | data formatting | bytes 393216
where the time goes:
time: 102 us; the launch traced here: 101 us
  Pallas kernels  95.5 us (94%)
  local copies, waits for them, and re-layouts  5.91 us (6%)
    pallas_call x1, Pallas kernels, local_kernel(): pl.pallas_call(functools.partial(block_kernel, sp_n, tp_n, capacity, conv...  95.5 us
    unnamed x3, local copies, waits for them, and re-layouts  4.5 us

commit v1 on v0

--- a/solution.py
+++ b/solution.py
@@ -120,7 +120,7 @@
 
 
 HALO = 32
-GROUPS = 2
+PAIR = 2
 TILE = 256
 F32 = jnp.float32
 BF16 = jnp.bfloat16
@@ -133,15 +133,14 @@
     taps,
     glu_value,
     glu_gate,
-    ids,
+    ids_row,
     conv_kernel,
     conv_gain,
     out_weight_hbm,
     residual_hbm,
     mix_gain,
-    routes_col,
     routes_row,
-    route_weights,
+    weights_row,
     gate_hbm,
     up_hbm,
     down_hbm,
@@ -152,9 +151,11 @@
     w_gate,
     w_up,
     w_down,
-    halo_v,
-    halo_g,
-    halo_i,
+    rim_out,
+    rim_in,
+    rim_ids,
+    by_row,
+    by_col,
     ext,
     ext_ids,
     fil,
@@ -202,12 +203,25 @@
     y = tp // 2
     core = tp % 2
     partner = y * 2 + (1 - core)
-    group_d = sp_n // GROUPS
-    group_rows = group_d * capacity
+    groups = sp_n // PAIR
+    group_rows = PAIR * capacity
     pending = []
 
     def y_at(k):
         return lax.rem(y + k, y_n)
+
+    near = list(range(PAIR, sp_n // 2))
+    far = sorted(range(sp_n // 2, sp_n), key=lambda r: (r % 2, r))
+    rest = [(2 * i + 1) / len(far) for i in range(len(far))], [(2 * i + 1) / len(near) for i in range(len(near))]
+    turns = list(range(PAIR)) + [r for _, r in sorted(zip(rest[0] + rest[1], far + near))]
+
+    def peer(p):
+        to, bit = sp, 1
+        while bit < sp_n:
+            if turns[p] & bit:
+                to = to + bit - 2 * bit * lax.rem(lax.div(sp, bit), 2)
+            bit *= 2
+        return to
 
     def feat_cols(block):
         return pl.ds(pl.multiple_of(block * feat, feat), feat)
@@ -255,26 +269,21 @@
             barrier, inc=1, device_id={"tp": lax.rem(tp + k, tp_n)},
             device_id_type=pl.DeviceIdType.MESH,
         )
-    pl.semaphore_wait(barrier, sp_n + tp_n - 2)
-
-    right = lax.rem(sp + 1, sp_n)
-    rim = pl.ds(tok - HALO, HALO)
-    halo = (
-        (glu_value, halo_v),
-        (glu_gate, halo_g),
-        (ids, halo_i),
-    )
-    for i, (src, dst) in enumerate(halo):
-        send(src.at[rim], dst, halo_sem.at[0, i], halo_sem.at[1, i], "sp", right)
-
-    def gated(value, gate):
-        value = value.astype(F32)
-        return (value * jax.nn.sigmoid(gate.astype(F32))).astype(BF16).astype(F32)
-
-    ext[HALO:, :] = gated(glu_value[...], glu_gate[...])
-    ext_ids[HALO:, :] = ids[...]
-
-    experts = sp_n
+
+    lanes = 128
+    wide = by_row.shape[1]
+    by_row[...] = jnp.zeros_like(by_row)
+    by_row[0:1, 0:tok] = ids_row[...].astype(F32)
+    by_row[1:3, 0:tok] = routes_row[...].astype(F32)
+    by_row[3:5, 0:tok] = weights_row[...]
+    by_col[...] = jnp.concatenate([by_row[...], jnp.zeros((lanes - 8, wide), F32)], 0).T[:tok]
+    ext_ids[HALO:, :] = jnp.broadcast_to(by_col[:, 0:1].astype(jnp.int32), (tok, lanes))
+
+    value = glu_value[...].astype(F32)
+    gated = (value * jax.nn.sigmoid(glu_gate[...].astype(F32))).astype(BF16)
+    ext[HALO:, :] = gated.astype(F32)
+    rim_out[...] = gated[tok - HALO :]
+
     lower = (
         lax.broadcasted_iota(jnp.int32, (tok, tok), 1)
         < lax.broadcasted_iota(jnp.int32, (tok, tok), 0)
@@ -283,50 +292,80 @@
         lax.broadcasted_iota(jnp.int32, (tok, tok), 0)
         < lax.broadcasted_iota(jnp.int32, (tok, tok), 1)
     )
-    lanes = 128
     e_lane = lax.broadcasted_iota(jnp.int32, (tok, lanes), 1)
-    rel_col = lax.rem(routes_col[...] - sp + experts, experts)
-    m0 = (rel_col[:, 0:1] == e_lane).astype(F32)
-    m1 = (rel_col[:, 1:2] == e_lane).astype(F32)
+    one_lane = lax.broadcasted_iota(jnp.int32, (1, lanes), 1)
+    subs = -(-sp_n // 16) * 16
+    e_sub = lax.broadcasted_iota(jnp.int32, (subs, tok), 0)
+    lane_expert = jnp.full((1, lanes), -1, jnp.int32)
+    sub_expert = jnp.full((subs, tok), -1, jnp.int32)
+    for r in range(sp_n):
+        lane_expert = jnp.where(one_lane == r, peer(r), lane_expert)
+        sub_expert = jnp.where(e_sub == r, peer(r), sub_expert)
+    lane_expert = lane_expert.astype(F32)
+    m0 = (by_col[:, 1:2] == lane_expert).astype(F32)
+    m1 = (by_col[:, 2:3] == lane_expert).astype(F32)
     rank = jnp.dot(lower.astype(F32).astype(BF16), (m0 + m1).astype(BF16), preferred_element_type=F32)
     place = rank + (e_lane * capacity).astype(F32)
     slot_col0 = jnp.sum(m0 * place, 1, keepdims=True).astype(jnp.int32)
     slot_col1 = jnp.sum(m1 * place, 1, keepdims=True).astype(jnp.int32)
-    e_sub = lax.broadcasted_iota(jnp.int32, (lanes, tok), 0)
-    rel_row = lax.rem(routes_row[...] - sp + experts, experts)
-    n0 = (rel_row[0:1, :] == e_sub).astype(F32)
-    n1 = (rel_row[1:2, :] == e_sub).astype(F32)
+    n0 = (routes_row[0:1, :] == sub_expert).astype(F32)
+    n1 = (routes_row[1:2, :] == sub_expert).astype(F32)
     rank_r = jnp.dot((n0 + n1).astype(BF16), upper.astype(F32).astype(BF16), preferred_element_type=F32)
     place_r = rank_r + (e_sub * capacity).astype(F32)
     slot_row0 = jnp.sum(n0 * place_r, 0, keepdims=True).astype(jnp.int32)
     slot_row1 = jnp.sum(n1 * place_r, 0, keepdims=True).astype(jnp.int32)
 
-    for i, (_, dst) in enumerate(halo):
-        arrived(dst, halo_sem.at[1, i], halo_sem.at[0, i], "sp", right)
-    first = jnp.where(sp == 0, 1, 0)
-    ext[:HALO, :] = gated(halo_v[...], halo_g[...])
-    ext_ids[:HALO, :] = halo_i[...] * (1 - first) - first
+    pl.semaphore_wait(barrier, sp_n + tp_n - 2)
+
+    right = lax.rem(sp + 1, sp_n)
+    halo = [
+        remote(src, dst, halo_sem.at[0, i], halo_sem.at[1, i], "sp", right)
+        for i, (src, dst) in enumerate(
+            ((rim_out, rim_in), (ext_ids.at[pl.ds(tok, HALO)], rim_ids))
+        )
+    ]
+
+    @pl.when(sp < sp_n - 1)
+    def _():
+        for copy in halo:
+            copy.start()
 
     kern = conv_kernel[...].astype(F32)
-    step = 32
     lane_blocks = chan // lanes
-    for at in range(0, tok, step):
-        own = ids[at : at + step, :]
-        acc = [jnp.zeros((step, lanes), F32) for _ in range(lane_blocks)]
+
+    def convolve(at):
+        own = ext_ids[HALO + at : 2 * HALO + at, :]
+        acc = [jnp.zeros((HALO, lanes), F32) for _ in range(lane_blocks)]
         for lag in range(taps):
             begin = HALO + at - lag
-            same = ext_ids[begin : begin + step, :] == own
+            same = ext_ids[begin : begin + HALO, :] == own
             for b in range(lane_blocks):
-                part = ext[begin : begin + step, b * lanes : (b + 1) * lanes]
+                part = ext[begin : begin + HALO, b * lanes : (b + 1) * lanes]
                 acc[b] = acc[b] + jnp.where(same, part, 0.0) * kern[lag : lag + 1, b * lanes : (b + 1) * lanes]
         for b in range(lane_blocks):
-            fil[at : at + step, b * lanes : (b + 1) * lanes] = acc[b]
+            fil[at : at + HALO, b * lanes : (b + 1) * lanes] = acc[b]
+
+    for at in range(HALO, tok, HALO):
+        convolve(at)
+
+    @pl.when(sp == 0)
+    def _():
+        ext[:HALO, :] = jnp.zeros((HALO, chan), F32)
+        ext_ids[:HALO, :] = jnp.full((HALO, lanes), -1, jnp.int32)
+
+    @pl.when(sp > 0)
+    def _():
+        for copy in halo:
+            copy.wait_recv()
+        ext[:HALO, :] = rim_in[...].astype(F32)
+        ext_ids[:HALO, :] = rim_ids[...]
+
+    convolve(0)
 
     def stats(i, value, width):
         row_sum = jnp.sum(value, 1, keepdims=True)
         row_square = jnp.sum(value * value, 1, keepdims=True)
         packed = jnp.where(e_lane == 0, row_sum, jnp.where(e_lane == 1, row_square, 0.0))
-        wide = stat_out.shape[2]
         packed = jnp.concatenate([packed, jnp.zeros((wide - tok, lanes), F32)], 0)
         stat_out[i] = packed.T[:8]
         for k in range(1, tp_n):
@@ -401,142 +440,140 @@
             block = rows_in.at[2 * y_at(y_n - k) + 1 - core, d]
             arrived(block, ag_recv.at[y_n - 1 + k, d], ag_send.at[y_n - 1 + k, d], "tp", partner)
 
-    for d in list(range(1, sp_n)) + [0]:
-        s_at = lax.broadcasted_iota(jnp.int32, (capacity, tok), 0) + d * capacity
+    def dispatch(p):
+        s_at = lax.broadcasted_iota(jnp.int32, (capacity, tok), 0) + p * capacity
         table = jnp.logical_or(s_at == slot_row0, s_at == slot_row1).astype(F32).astype(BF16)
         block = jnp.dot(table, mixed[...], preferred_element_type=F32).astype(BF16)
-        if d:
-            outbox[d] = block
+        if p:
+            outbox[p] = block
             send(
-                outbox.at[d], rows_in.at[tp, d], disp_send.at[d], disp_recv.at[d],
-                "sp", lax.rem(sp + d, sp_n),
+                outbox.at[p], rows_in.at[tp, p], disp_send.at[p], disp_recv.at[p],
+                "sp", peer(p),
             )
         else:
             rows_in[tp, 0] = block
-
-    def landed(d):
-        if d:
-            arrived(rows_in.at[tp, d], disp_recv.at[d], disp_send.at[d], "sp", right)
-        spread(d)
-
-    def gate_up(g, lo, hi):
-        @pl.loop(lo, hi)
-        def _(n):
-            cols = pl.ds(pl.multiple_of(n * TILE, TILE), TILE)
-            rows = [
-                rows_in[j, g * group_d : (g + 1) * group_d].reshape(group_rows, feat)
-                for j in range(tp_n)
-            ]
-            x = jnp.concatenate(rows, 1)
-            gate = jnp.dot(x, w_gate[:, cols], preferred_element_type=F32)
-            up = jnp.dot(x, w_up[:, cols], preferred_element_type=F32)
-            hidden[g, :, cols] = (gate * jax.nn.sigmoid(gate) * up).astype(BF16)
-
-    def down_tile(g, block, t):
-        cols = pl.ds(pl.multiple_of(block * feat + t * TILE, TILE), TILE)
-        return jnp.dot(hidden[g], w_down[:, cols], preferred_element_type=F32)
-
-    def down(g, between=lambda: None):
+            spread(0)
+
+    def landed(p):
+        arrived(rows_in.at[tp, p], disp_recv.at[p], disp_send.at[p], "sp", right)
+        spread(p)
+
+    def gate_up(g, n):
+        cols = pl.ds(n * TILE, TILE)
+        rows = [
+            rows_in[j, PAIR * g : PAIR * (g + 1)].reshape(group_rows, feat) for j in range(tp_n)
+        ]
+        x = jnp.concatenate(rows, 1)
+        gate = jnp.dot(x, w_gate[:, cols], preferred_element_type=F32)
+        up = jnp.dot(x, w_up[:, cols], preferred_element_type=F32)
+        hidden[g, :, cols] = (gate * jax.nn.sigmoid(gate) * up).astype(BF16)
+
+    def down(g):
+        def part(block):
+            return jnp.dot(hidden[g], w_down[:, feat_cols(block)], preferred_element_type=F32)
+
         for k in order:
-            block = 2 * y_at(k) + 1 - core
-
-            @pl.loop(0, feat // TILE)
-            def _(t):
-                cols = pl.ds(pl.multiple_of(t * TILE, TILE), TILE)
-                part_pp[g, k, :, cols] = down_tile(g, block, t).astype(BF16)
-
+            part_pp[g, k] = part(2 * y_at(k) + 1 - core).astype(BF16)
             send(
                 part_pp.at[g, k], part_a.at[g, k], part_send.at[g, k], part_recv.at[g, k],
                 "tp", partner,
             )
-        between()
-        for k in order:
-            block = 2 * y_at(k) + core
+            part_own[g, k] = part(2 * y_at(k) + core)
+
+    def cross(g):
+        for k in order[:-1]:
             arrived(part_a.at[g, k], part_recv.at[g, k], part_send.at[g, k], "tp", partner)
-
-            @pl.loop(0, feat // TILE)
-            def _(t):
-                cols = pl.ds(pl.multiple_of(t * TILE, TILE), TILE)
-                value = down_tile(g, block, t) + part_a[g, k, :, cols].astype(F32)
-                if k:
-                    part_s[g, k, :, cols] = value.astype(BF16)
-                else:
-                    part_own[g, :, cols] = value
-
-            for i in range(group_d if k else 0):
+            part_s[g, k] = (part_own[g, k] + part_a[g, k].astype(F32)).astype(BF16)
+            for i in range(PAIR):
                 rows = pl.ds(i * capacity, capacity)
                 send(
                     part_s.at[g, k, rows], part_b.at[g, k, rows],
                     cross_send.at[g, k, i], cross_recv.at[g, k, i],
                     "tp", 2 * y_at(k) + core,
                 )
-
-    def finish(g, i):
-        d = g * group_d + i
+        arrived(part_a.at[g, 0], part_recv.at[g, 0], part_send.at[g, 0], "tp", partner)
+
+    def finish(p):
+        g, i = p // PAIR, p % PAIR
         rows = pl.ds(i * capacity, capacity)
-        value = part_own[g, rows, :]
+        value = part_own[g, 0, rows, :] + part_a[g, 0, rows, :].astype(F32)
         for k in range(1, y_n):
             arrived(
                 part_b.at[g, k, rows], cross_recv.at[g, k, i], cross_send.at[g, k, i],
                 "tp", partner,
             )
             value = value + part_b[g, k, rows, :].astype(F32)
-        if d:
-            back_out[d] = value.astype(BF16)
+        if p:
+            back_out[p] = value.astype(BF16)
             send(
-                back_out.at[d], back_in.at[d], back_send.at[d], back_recv.at[d],
-                "sp", lax.rem(sp - d + sp_n, sp_n),
+                back_out.at[p], back_in.at[p], back_send.at[p], back_recv.at[p],
+                "sp", peer(p),
             )
         else:
             back_in[0] = value.astype(BF16)
 
-    for d in range(group_d):
-        landed(d)
-        if d:
-            pass_on(d - 1)
-    pass_on(group_d - 1)
-    for d in range(group_d):
-        gathered(d)
+    tiles = ff // TILE
+    early = PAIR + 3
+    for p in range(early):
+        dispatch(p)
+    pass_on(0)
+    for p in range(early, sp_n):
+        dispatch(p)
+    landed(1)
+    landed(2)
+    pass_on(1)
     loads[2].wait()
     loads[3].wait()
-    tiles = ff // TILE
-    for n in range(tiles):
-        gate_up(0, n, n + 1)
-        if n < group_d:
-            landed(group_d + n)
-        if 1 <= n <= group_d:
-            pass_on(group_d + n - 1)
-    for i in range(min(tiles, group_d), group_d):
-        landed(group_d + i)
-    for i in range(min(max(tiles - 1, 0), group_d), group_d):
-        pass_on(group_d + i)
-    loads[4].wait()
-    down(0)
-    for d in range(group_d, sp_n):
-        gathered(d)
-    half = tiles // 2
-    gate_up(1, 0, half)
-    finish(0, 0)
-    gate_up(1, half, tiles)
-    for i in range(1, group_d // 2):
-        finish(0, i)
-    down(1, lambda: [finish(0, i) for i in range(max(1, group_d // 2), group_d)])
-    for i in range(group_d):
-        finish(1, i)
-
-    for d in range(1, sp_n):
-        arrived(back_in.at[d], back_recv.at[d], back_send.at[d], "sp", right)
+    for g in range(groups):
+        for p in range(PAIR * g, PAIR * (g + 1)):
+            gathered(p)
+        gaps = -(-tiles // 2)
+        steps = [[] for _ in range(gaps + 1)]
+
+        def put(gap, step, p):
+            if p < sp_n:
+                steps[min(gap, gaps)].append(functools.partial(step, p))
+
+        put(0, landed, PAIR * g + 3)
+        put(1, pass_on, PAIR * g + 2)
+        put(1, landed, PAIR * g + 4)
+        put(gaps, pass_on, PAIR * g + 3)
+        if g >= 2:
+            put(1, finish, PAIR * (g - 2))
+            put(2, finish, PAIR * (g - 2) + 1)
+        for n in range(tiles):
+            gate_up(g, n)
+            if n % 2 or n == tiles - 1:
+                for step in steps[n // 2]:
+                    step()
+        if g == 0:
+            loads[4].wait()
+        down(g)
+        cross(g)
+        for step in steps[gaps]:
+            step()
+    for g in range(groups - 2, groups):
+        for i in range(PAIR):
+            finish(PAIR * g + i)
+
+    for p in range(1, sp_n):
+        arrived(back_in.at[p], back_recv.at[p], back_send.at[p], "sp", right)
     slots = sp_n * capacity
     returned = back_in[...].reshape(slots, feat)
     s_lane = lax.broadcasted_iota(jnp.int32, (tok, slots), 1)
     pick0 = jnp.dot((s_lane == slot_col0).astype(F32).astype(BF16), returned, preferred_element_type=F32)
     pick1 = jnp.dot((s_lane == slot_col1).astype(F32).astype(BF16), returned, preferred_element_type=F32)
-    moe = route_weights[:, 0:1] * pick0 + route_weights[:, 1:2] * pick1
+    moe = by_col[:, 3:4] * pick0 + by_col[:, 4:5] * pick1
     pre = residual_alpha * mixed[...].astype(F32) + moe
     mean, scale = stats(2, pre, feat * tp_n)
     out[...] = ((pre - mean) * scale * final_gain[...]).astype(BF16)
     for copy in pending:
         copy.wait_send()
+
+    @pl.when(sp < sp_n - 1)
+    def _():
+        for copy in halo:
+            copy.wait_send()
 
 
 def local_kernel(
@@ -561,7 +598,7 @@
     width, ff = expert_gate.shape[1:]
     capacity = 4 * tok // sp_n
     y_n = tp_n // 2
-    rows = sp_n // GROUPS * capacity
+    groups, rows = sp_n // PAIR, PAIR * capacity
     wide = -(-tok // 128) * 128
     vmem = pl.BlockSpec(memory_space=pltpu.VMEM)
     hbm = pl.BlockSpec(memory_space=pl.ANY)
@@ -575,6 +612,8 @@
         pltpu.VMEM((HALO, chan), BF16),
         pltpu.VMEM((HALO, chan), BF16),
         pltpu.VMEM((HALO, 128), jnp.int32),
+        pltpu.VMEM((8, wide), F32),
+        pltpu.VMEM((tok, 128), F32),
         pltpu.VMEM((HALO + tok, chan), F32),
         pltpu.VMEM((HALO + tok, 128), jnp.int32),
         pltpu.VMEM((tok, chan), F32),
@@ -587,16 +626,16 @@
         pltpu.VMEM((tok, feat), BF16),
         pltpu.VMEM((sp_n, capacity, feat), BF16),
         pltpu.VMEM((tp_n, sp_n, capacity, feat), BF16),
-        pltpu.VMEM((GROUPS, rows, ff), BF16),
-        pltpu.VMEM((GROUPS, y_n, rows, feat), BF16),
-        pltpu.VMEM((GROUPS, y_n, rows, feat), BF16),
-        pltpu.VMEM((GROUPS, y_n, rows, feat), BF16),
-        pltpu.VMEM((GROUPS, y_n, rows, feat), BF16),
-        pltpu.VMEM((GROUPS, rows, feat), F32),
+        pltpu.VMEM((groups, rows, ff), BF16),
+        pltpu.VMEM((groups, y_n, rows, feat), BF16),
+        pltpu.VMEM((groups, y_n, rows, feat), BF16),
+        pltpu.VMEM((groups, y_n, rows, feat), BF16),
+        pltpu.VMEM((groups, y_n, rows, feat), BF16),
+        pltpu.VMEM((groups, y_n, rows, feat), F32),
         pltpu.VMEM((sp_n, capacity, feat), BF16),
         pltpu.VMEM((sp_n, capacity, feat), BF16),
         dma((5,)),
-        dma((2, 3)),
+        dma((2, 2)),
         dma((3, tp_n)),
         dma((3, tp_n)),
         dma((2, y_n)),
@@ -605,17 +644,17 @@
         dma((sp_n,)),
         dma((2 * y_n - 1, sp_n)),
         dma((2 * y_n - 1, sp_n)),
-        dma((GROUPS, y_n)),
-        dma((GROUPS, y_n)),
-        dma((GROUPS, y_n, sp_n // GROUPS)),
-        dma((GROUPS, y_n, sp_n // GROUPS)),
+        dma((groups, y_n)),
+        dma((groups, y_n)),
+        dma((groups, y_n, PAIR)),
+        dma((groups, y_n, PAIR)),
         dma((sp_n,)),
         dma((sp_n,)),
     ]
     return pl.pallas_call(
         functools.partial(block_kernel, sp_n, tp_n, capacity, conv_kernel.shape[0]),
         out_shape=jax.ShapeDtypeStruct((tok, feat), BF16),
-        in_specs=[vmem] * 5 + [hbm] * 2 + [vmem] * 4 + [hbm] * 3 + [vmem],
+        in_specs=[vmem] * 5 + [hbm] * 2 + [vmem] * 3 + [hbm] * 3 + [vmem],
         out_specs=vmem,
         scratch_shapes=scratch,
         compiler_params=pltpu.CompilerParams(
@@ -624,15 +663,14 @@
     )(
         glu_value,
         glu_gate,
-        jnp.broadcast_to(doc_ids[:, None], (tok, 128)),
+        doc_ids[None, :],
         conv_kernel,
         conv_gain[None, :],
         out_weight,
         residual,
         mix_gain[None, :],
-        routes,
         routes.T,
-        route_weights,
+        route_weights.T,
         expert_gate,
         expert_up,
         expert_down,
@@ -654,8 +692,8 @@
         and args[3].shape[0] <= HALO
         and tp_n % 2 == 0
         and tp_n > 2
-        and sp_n % GROUPS == 0
-        and sp_n > GROUPS
+        and sp_n & (sp_n - 1) == 0
+        and sp_n > 2 * PAIR
         and sp_n <= 128
         and args[10].shape[0] == 1
     )

time: 102 us -> 83.7 us (0.82)
  Pallas kernels: 95.5 us -> 81.8 us
  local copies, waits for them, and re-layouts: 5.91 us -> 1.62 us
    pallas_call x1, Pallas kernels: 95.5 us -> 81.8 us  [local_kernel(): pl.pallas_call(functools.partial(block_kernel, sp_n, tp_n, capacity, conv...]
    unnamed x3 -> x1, local copies, waits for them, and re-layouts: 4.5 us -> 1.62 us
    broadcast_in_dim x1 -> x0, local copies, waits for them, and re-layouts: 1.41 us -> none  [local_kernel(): jnp.broadcast_to(doc_ids[:, None], (tok, 128))]
where the time goes in v1:
time: 83.7 us; the launch traced here: 83.4 us
  Pallas kernels  81.8 us (98%)
  local copies, waits for them, and re-layouts  1.62 us (2%)
    pallas_call x1, Pallas kernels, local_kernel(): pl.pallas_call(functools.partial(block_kernel, sp_n, tp_n, capacity, conv...  81.8 us

profile of v1, /device:TPU:0, one launch (start us, length us, event | category | flops | bytes accessed | tf_op | source)
XLA Modules:
  0.0 83.4 jit_solution(18130348331572060397)
XLA Ops:
  0.0 81.8 %shard_map.136 = bf16[192,512]{1,0:T(8,128)(2,1)} custom-call(bf16[192,256]{1,0:T(8,128)(2,1)} %glu_value.1, bf16[192,256]{1,0:T(8,128)(2,1)} %glu_gate.1, s32[1,192]{1,0:T(1,128)} %bitcast.10, bf16[31,256]{1,0:T(8,128)(2,1)} %conv_kernel.1, f32[1,256]{1,0:T(1,128)} %bitcast.11, bf16[256,2048]{1,0:T(8,128)(2,1)} %out_weight_hbm.1, ...), custom_call_target="tpu_custom_call" | custom-call | tf_op jit(solution)/shard_map/pallas_call | solution.py:654
  81.8 1.6 %copy.16 = bf16[192,512]{1,0:T(8,128)(2,1)} copy(bf16[192,512]{1,0:T(8,128)(2,1)} %shard_map.136) | data formatting | bytes 393216

commit v2 on v1

--- a/solution.py
+++ b/solution.py
@@ -122,6 +122,15 @@
 HALO = 32
 PAIR = 2
 TILE = 256
+TURNS = (0, 4, 1, 6, 2, 5, 7, 3)
+PLAN = (
+    ("D0", "D1", "D2", "D4", "F0", "D3", "D7", "L2", "D5", "D6", "L4", "L1", "F2", "F1",),
+    (("L3",), ("F4", "L7",), (), ("F3", "L5",)),
+    (("X0",), ("F7", "L6",), (), ("F5",)),
+    (("X1",), (), ("R0", "R1",), ("F6",)),
+    (("X2",), (), ("R3", "R2",), ()),
+    ("X3", "R5", "R4", "R6", "R7",),
+)
 F32 = jnp.float32
 BF16 = jnp.bfloat16
 
@@ -131,21 +140,30 @@
     tp_n,
     capacity,
     taps,
+    glu_value_hbm,
+    glu_gate_hbm,
+    ids_hbm,
+    conv_kernel_hbm,
+    conv_gain_hbm,
+    out_weight_hbm,
+    residual_hbm,
+    mix_gain_hbm,
+    routes_hbm,
+    weights_hbm,
+    gate_hbm,
+    up_hbm,
+    down_hbm,
+    final_gain_hbm,
+    out,
     glu_value,
     glu_gate,
     ids_row,
     conv_kernel,
     conv_gain,
-    out_weight_hbm,
-    residual_hbm,
     mix_gain,
     routes_row,
     weights_row,
-    gate_hbm,
-    up_hbm,
-    down_hbm,
     final_gain,
-    out,
     w_out,
     resid,
     w_gate,
@@ -176,6 +194,7 @@
     part_own,
     back_out,
     back_in,
+    small_sem,
     load_sem,
     halo_sem,
     stat_send,
@@ -193,9 +212,8 @@
     back_send,
     back_recv,
 ):
-    tok = glu_value.shape[0]
-    chan = glu_value.shape[1]
-    feat = final_gain.shape[1]
+    tok, chan = glu_value.shape
+    feat = final_gain_hbm.shape[1]
     ff = hidden.shape[2]
     y_n = tp_n // 2
     sp = lax.axis_index("sp")
@@ -210,15 +228,10 @@
     def y_at(k):
         return lax.rem(y + k, y_n)
 
-    near = list(range(PAIR, sp_n // 2))
-    far = sorted(range(sp_n // 2, sp_n), key=lambda r: (r % 2, r))
-    rest = [(2 * i + 1) / len(far) for i in range(len(far))], [(2 * i + 1) / len(near) for i in range(len(near))]
-    turns = list(range(PAIR)) + [r for _, r in sorted(zip(rest[0] + rest[1], far + near))]
-
     def peer(p):
         to, bit = sp, 1
         while bit < sp_n:
-            if turns[p] & bit:
+            if TURNS[p] & bit:
                 to = to + bit - 2 * bit * lax.rem(lax.div(sp, bit), 2)
             bit *= 2
         return to
@@ -244,6 +257,37 @@
     def arrived(dst, recv, send_sem, axis, to):
         remote(dst, dst, send_sem, recv, axis, to).wait_recv()
 
+    barrier = pltpu.get_barrier_semaphore()
+    for k in range(1, sp_n):
+        pl.semaphore_signal(
+            barrier, inc=1, device_id={"sp": lax.rem(sp + k, sp_n)},
+            device_id_type=pl.DeviceIdType.MESH,
+        )
+    for k in range(1, tp_n):
+        pl.semaphore_signal(
+            barrier, inc=1, device_id={"tp": lax.rem(tp + k, tp_n)},
+            device_id_type=pl.DeviceIdType.MESH,
+        )
+
+    smalls = []
+    for i, (src, dst) in enumerate(
+        (
+            (ids_hbm, ids_row),
+            (routes_hbm, routes_row),
+            (weights_hbm, weights_row),
+            (glu_value_hbm, glu_value),
+            (glu_gate_hbm, glu_gate),
+            (conv_kernel_hbm, conv_kernel),
+            (conv_gain_hbm, conv_gain),
+            (mix_gain_hbm, mix_gain),
+            (final_gain_hbm, final_gain),
+        )
+    ):
+        copy = pltpu.make_async_copy(src, dst, small_sem.at[i])
+        copy.start()
+        smalls.append(copy)
+    for copy in smalls:
+        copy.wait()
     loads = []
     for i, (src, dst) in enumerate(
         (
@@ -257,18 +301,6 @@
         copy = pltpu.make_async_copy(src, dst, load_sem.at[i])
         copy.start()
         loads.append(copy)
-
-    barrier = pltpu.get_barrier_semaphore()
-    for k in range(1, sp_n):
-        pl.semaphore_signal(
-            barrier, inc=1, device_id={"sp": lax.rem(sp + k, sp_n)},
-            device_id_type=pl.DeviceIdType.MESH,
-        )
-    for k in range(1, tp_n):
-        pl.semaphore_signal(
-            barrier, inc=1, device_id={"tp": lax.rem(tp + k, tp_n)},
-            device_id_type=pl.DeviceIdType.MESH,
-        )
 
     lanes = 128
     wide = by_row.shape[1]
@@ -484,7 +516,7 @@
         for k in order[:-1]:
             arrived(part_a.at[g, k], part_recv.at[g, k], part_send.at[g, k], "tp", partner)
             part_s[g, k] = (part_own[g, k] + part_a[g, k].astype(F32)).astype(BF16)
-            for i in range(PAIR):
+            for i in ((0, 1) if g == groups - 1 else (1, 0)):
                 rows = pl.ds(i * capacity, capacity)
                 send(
                     part_s.at[g, k, rows], part_b.at[g, k, rows],
@@ -513,57 +545,40 @@
             back_in[0] = value.astype(BF16)
 
     tiles = ff // TILE
-    early = PAIR + 3
-    for p in range(early):
-        dispatch(p)
-    pass_on(0)
-    for p in range(early, sp_n):
-        dispatch(p)
-    landed(1)
-    landed(2)
-    pass_on(1)
+    early = PLAN[0]
+    do = dict(D=dispatch, L=landed, F=pass_on, R=finish, X=cross)
+
+    def act(text):
+        for word in text:
+            do[word[0]](int(word[1:]))
+
+    act(early)
     loads[2].wait()
     loads[3].wait()
     for g in range(groups):
         for p in range(PAIR * g, PAIR * (g + 1)):
             gathered(p)
-        gaps = -(-tiles // 2)
-        steps = [[] for _ in range(gaps + 1)]
-
-        def put(gap, step, p):
-            if p < sp_n:
-                steps[min(gap, gaps)].append(functools.partial(step, p))
-
-        put(0, landed, PAIR * g + 3)
-        put(1, pass_on, PAIR * g + 2)
-        put(1, landed, PAIR * g + 4)
-        put(gaps, pass_on, PAIR * g + 3)
-        if g >= 2:
-            put(1, finish, PAIR * (g - 2))
-            put(2, finish, PAIR * (g - 2) + 1)
         for n in range(tiles):
             gate_up(g, n)
             if n % 2 or n == tiles - 1:
-                for step in steps[n // 2]:
-                    step()
+                act(PLAN[1 + g][n // 2])
         if g == 0:
             loads[4].wait()
         down(g)
-        cross(g)
-        for step in steps[gaps]:
-            step()
-    for g in range(groups - 2, groups):
-        for i in range(PAIR):
-            finish(PAIR * g + i)
-
-    for p in range(1, sp_n):
-        arrived(back_in.at[p], back_recv.at[p], back_send.at[p], "sp", right)
-    slots = sp_n * capacity
-    returned = back_in[...].reshape(slots, feat)
-    s_lane = lax.broadcasted_iota(jnp.int32, (tok, slots), 1)
-    pick0 = jnp.dot((s_lane == slot_col0).astype(F32).astype(BF16), returned, preferred_element_type=F32)
-    pick1 = jnp.dot((s_lane == slot_col1).astype(F32).astype(BF16), returned, preferred_element_type=F32)
-    moe = by_col[:, 3:4] * pick0 + by_col[:, 4:5] * pick1
+        act(PLAN[1 + g][3])
+    act(PLAN[-1])
+
+    def combine(lo, hi):
+        for p in range(max(lo, 1), hi):
+            arrived(back_in.at[p], back_recv.at[p], back_send.at[p], "sp", right)
+        slots = (hi - lo) * capacity
+        rows = back_in[lo:hi].reshape(slots, feat)
+        s_lane = lax.broadcasted_iota(jnp.int32, (tok, slots), 1) + lo * capacity
+        pick0 = jnp.dot((s_lane == slot_col0).astype(F32).astype(BF16), rows, preferred_element_type=F32)
+        pick1 = jnp.dot((s_lane == slot_col1).astype(F32).astype(BF16), rows, preferred_element_type=F32)
+        return by_col[:, 3:4] * pick0 + by_col[:, 4:5] * pick1
+
+    moe = combine(0, sp_n - PAIR) + combine(sp_n - PAIR, sp_n)
     pre = residual_alpha * mixed[...].astype(F32) + moe
     mean, scale = stats(2, pre, feat * tp_n)
     out[...] = ((pre - mean) * scale * final_gain[...]).astype(BF16)
@@ -604,6 +619,15 @@
     hbm = pl.BlockSpec(memory_space=pl.ANY)
     dma = pltpu.SemaphoreType.DMA
     scratch = [
+        pltpu.VMEM((tok, chan), BF16),
+        pltpu.VMEM((tok, chan), BF16),
+        pltpu.VMEM((1, tok), jnp.int32),
+        pltpu.VMEM(conv_kernel.shape, BF16),
+        pltpu.VMEM((1, chan), F32),
+        pltpu.VMEM((1, width), F32),
+        pltpu.VMEM((2, tok), jnp.int32),
+        pltpu.VMEM((2, tok), F32),
+        pltpu.VMEM((1, feat), F32),
         pltpu.VMEM((chan, width), BF16),
         pltpu.VMEM((tok, feat), BF16),
         pltpu.VMEM((width, ff), BF16),
@@ -634,6 +658,7 @@
         pltpu.VMEM((groups, y_n, rows, feat), F32),
         pltpu.VMEM((sp_n, capacity, feat), BF16),
         pltpu.VMEM((sp_n, capacity, feat), BF16),
+        dma((9,)),
         dma((5,)),
         dma((2, 2)),
         dma((3, tp_n)),
@@ -653,8 +678,8 @@
     ]
     return pl.pallas_call(
         functools.partial(block_kernel, sp_n, tp_n, capacity, conv_kernel.shape[0]),
-        out_shape=jax.ShapeDtypeStruct((tok, feat), BF16),
-        in_specs=[vmem] * 5 + [hbm] * 2 + [vmem] * 3 + [hbm] * 3 + [vmem],
+        out_shape=pltpu.VMEM((tok, feat), BF16),
+        in_specs=[hbm] * 14,
         out_specs=vmem,
         scratch_shapes=scratch,
         compiler_params=pltpu.CompilerParams(
@@ -692,9 +717,8 @@
         and args[3].shape[0] <= HALO
         and tp_n % 2 == 0
         and tp_n > 2
-        and sp_n & (sp_n - 1) == 0
-        and sp_n > 2 * PAIR
-        and sp_n <= 128
+        and sp_n == len(TURNS)
+        and -(-ff // (2 * TILE)) <= len(PLAN[1]) - 1
         and args[10].shape[0] == 1
     )
     return (local_kernel if aligned else local_plain)(*args)

time: 83.7 us -> 77.9 us (0.931)
  Pallas kernels: 81.8 us -> 77.1 us
  local copies, waits for them, and re-layouts: 1.62 us -> 0.68 us
    pallas_call x1, Pallas kernels: 81.8 us -> 77.1 us  [local_kernel(): pl.pallas_call(functools.partial(block_kernel, sp_n, tp_n, capacity, conv...]
    unnamed x1, local copies, waits for them, and re-layouts: 1.62 us -> 0.68 us
where the time goes in v2:
time: 77.9 us; the launch traced here: 77.8 us
  Pallas kernels  77.1 us (99%)
    pallas_call x1, Pallas kernels, local_kernel(): pl.pallas_call(functools.partial(block_kernel, sp_n, tp_n, capacity, conv...  77.1 us

profile of v2, /device:TPU:0, one launch (start us, length us, event | category | flops | bytes accessed | tf_op | source)
XLA Modules:
  0.0 77.8 jit_solution(10824766277356416332)
XLA Ops:
  0.0 77.1 %shard_map.136 = bf16[192,512]{1,0:T(8,128)(2,1)S(1)} custom-call(bf16[192,256]{1,0:T(8,128)(2,1)} %glu_value_hbm.1, bf16[192,256]{1,0:T(8,128)(2,1)} %glu_gate_hbm.1, s32[1,192]{1,0:T(1,128)} %bitcast.10, bf16[31,256]{1,0:T(8,128)(2,1)} %conv_kernel_hbm.1, f32[1,256]{1,0:T(1,128)} %bitcast.11, bf16[256,2048]{1,0:T(8,128)(2,1)} %out_weight_hbm.1, ...), custom_call_target="tpu_custom_call" | custom-call | tf_op jit(solution)/shard_map/pallas_call | solution.py:679
  77.1 0.7 copy.16

commit v3 on v2

--- a/solution.py
+++ b/solution.py
@@ -120,16 +120,17 @@
 
 
 HALO = 32
-PAIR = 2
 TILE = 256
-TURNS = (0, 4, 1, 6, 2, 5, 7, 3)
+TURNS = (0, 4, 1, 6, 2, 5, 3, 7)
+SIZES = (1, 2, 2, 2, 1)
 PLAN = (
-    ("D0", "D1", "D2", "D4", "F0", "D3", "D7", "L2", "D5", "D6", "L4", "L1", "F2", "F1",),
-    (("L3",), ("F4", "L7",), (), ("F3", "L5",)),
-    (("X0",), ("F7", "L6",), (), ("F5",)),
-    (("X1",), (), ("R0", "R1",), ("F6",)),
-    (("X2",), (), ("R3", "R2",), ()),
-    ("X3", "R5", "R4", "R6", "R7",),
+    ("D0", "D1", "D2", "S0", "F0", "D3", "D4"),
+    ((), ("L2", "D6"), ("L1", "D5"), ("D7", "F2"), ("L4", "F1", "X0")),
+    ((), ("L3",), ("F4", "L6"), (), ("F3", "L5")),
+    (("X1",), (), ("F6", "L7"), ("R0",), ("F5", "R1")),
+    (("X2",), ("R2",), (), (), ("F7", "R3")),
+    (("X3",), ("R4",), (), (), ()),
+    ("X4", "R5", "R6", "R7"),
 )
 F32 = jnp.float32
 BF16 = jnp.bfloat16
@@ -183,7 +184,12 @@
     mix_a,
     mix_s,
     mix_b,
+    plain,
+    raw,
     mixed,
+    ready,
+    note_out,
+    note_in,
     outbox,
     rows_in,
     hidden,
@@ -201,6 +207,8 @@
     stat_recv,
     mix_send,
     mix_recv,
+    note_send,
+    note_recv,
     disp_send,
     disp_recv,
     ag_send,
@@ -221,8 +229,9 @@
     y = tp // 2
     core = tp % 2
     partner = y * 2 + (1 - core)
-    groups = sp_n // PAIR
-    group_rows = PAIR * capacity
+    groups = len(SIZES)
+    begins = [sum(SIZES[:g]) for g in range(groups)]
+    members = [range(begins[g], begins[g] + SIZES[g]) for g in range(groups)]
     pending = []
 
     def y_at(k):
@@ -340,6 +349,9 @@
     place = rank + (e_lane * capacity).astype(F32)
     slot_col0 = jnp.sum(m0 * place, 1, keepdims=True).astype(jnp.int32)
     slot_col1 = jnp.sum(m1 * place, 1, keepdims=True).astype(jnp.int32)
+    spaced = rank + (e_lane * lanes).astype(F32)
+    wide_col0 = jnp.sum(m0 * spaced, 1, keepdims=True).astype(jnp.int32)
+    wide_col1 = jnp.sum(m1 * spaced, 1, keepdims=True).astype(jnp.int32)
     n0 = (routes_row[0:1, :] == sub_expert).astype(F32)
     n1 = (routes_row[1:2, :] == sub_expert).astype(F32)
     rank_r = jnp.dot((n0 + n1).astype(BF16), upper.astype(F32).astype(BF16), preferred_element_type=F32)
@@ -394,7 +406,7 @@
 
     convolve(0)
 
-    def stats(i, value, width):
+    def stats_out(i, value):
         row_sum = jnp.sum(value, 1, keepdims=True)
         row_square = jnp.sum(value * value, 1, keepdims=True)
         packed = jnp.where(e_lane == 0, row_sum, jnp.where(e_lane == 1, row_square, 0.0))
@@ -405,14 +417,27 @@
                 stat_out.at[i], stat_in.at[i, k], stat_send.at[i, k], stat_recv.at[i, k],
                 "tp", lax.rem(tp + k, tp_n),
             )
+
+    def stats_in(i, width):
         total = stat_out[i]
         for k in range(1, tp_n):
             arrived(stat_in.at[i, k], stat_recv.at[i, k], stat_send.at[i, k], "tp", partner)
             total = total + stat_in[i, k]
-        total = jnp.concatenate([total, jnp.zeros((lanes - 8, wide), F32)], 0).T[:tok]
-        mean = total[:, 0:1] / width
-        var = total[:, 1:2] / width - mean * mean
+        mean = total[0:1] / width
+        var = total[1:2] / width - mean * mean
         return mean, lax.rsqrt(var + norm_eps)
+
+    row_of = lax.broadcasted_iota(jnp.int32, (8, wide), 0)
+
+    def columns(rows, count):
+        rows = jnp.concatenate([rows, jnp.zeros((lanes - 8, rows.shape[1]), F32)], 0)
+        return rows.T[:count]
+
+    def stats(i, value, width):
+        stats_out(i, value)
+        mean, scale = stats_in(i, width)
+        both = columns(jnp.where(row_of == 0, mean, jnp.where(row_of == 1, scale, 0.0)), tok)
+        return both[:, 0:1], both[:, 1:2]
 
     filtered = fil[...]
     mean, scale = stats(0, filtered, chan * tp_n)
@@ -444,8 +469,9 @@
     for k in range(1, y_n):
         arrived(mix_b.at[k], mix_recv.at[1, k], mix_send.at[1, k], "tp", partner)
         pre = pre + mix_b[k].astype(F32)
-    mean, scale = stats(1, pre, feat * tp_n)
-    mixed[...] = ((pre - mean) * scale * mix_gain[:, feat_cols(tp)]).astype(BF16)
+    plain[...] = pre
+    raw[...] = pre.astype(BF16)
+    stats_out(1, pre)
 
     def spread(d):
         block = rows_in.at[tp, d]
@@ -475,7 +501,7 @@
     def dispatch(p):
         s_at = lax.broadcasted_iota(jnp.int32, (capacity, tok), 0) + p * capacity
         table = jnp.logical_or(s_at == slot_row0, s_at == slot_row1).astype(F32).astype(BF16)
-        block = jnp.dot(table, mixed[...], preferred_element_type=F32).astype(BF16)
+        block = jnp.dot(table, raw[...], preferred_element_type=F32).astype(BF16)
         if p:
             outbox[p] = block
             send(
@@ -486,47 +512,86 @@
             rows_in[tp, 0] = block
             spread(0)
 
+    def describe(_):
+        mean, scale = stats_in(1, feat * tp_n)
+        both = columns(jnp.where(row_of == 0, mean, jnp.where(row_of == 1, scale, 0.0)), tok)
+        mixed[...] = (
+            (plain[...] - both[:, 0:1]) * both[:, 1:2] * mix_gain[:, feat_cols(tp)]
+        ).astype(BF16)
+        mean_top = mean.astype(BF16).astype(F32)
+        scale_top = scale.astype(BF16).astype(F32)
+        rows = jnp.zeros((8, wide), F32)
+        for at, row in enumerate((mean_top, mean - mean_top, scale_top, scale - scale_top)):
+            rows = jnp.where(row_of == at, row, rows)
+        w_lane = lax.broadcasted_iota(jnp.int32, (tok, sp_n * lanes), 1)
+        takes = jnp.logical_or(w_lane == wide_col0, w_lane == wide_col1).astype(F32).astype(BF16)
+        told = jnp.dot(rows[:, :tok].astype(BF16), takes, preferred_element_type=F32)
+        for p in range(sp_n):
+            block = told[:, p * lanes : (p + 1) * lanes]
+            if p:
+                note_out[p] = block
+                send(note_out.at[p], note_in.at[p], note_send.at[p], note_recv.at[p], "sp", peer(p))
+            else:
+                note_in[0] = block
+
+    def normalize(g, i, p):
+        if p:
+            arrived(note_in.at[p], note_recv.at[p], note_send.at[p], "sp", right)
+        note = columns(note_in[p], capacity)
+        mean = note[:, 0:1] + note[:, 1:2]
+        scale = note[:, 2:3] + note[:, 3:4]
+        for j in range(tp_n):
+            cols = pl.ds(j * feat, feat)
+            value = (rows_in[j, p].astype(F32) - mean) * scale * mix_gain[:, cols]
+            ready[i * capacity : (i + 1) * capacity, cols] = value.astype(BF16)
+
     def landed(p):
         arrived(rows_in.at[tp, p], disp_recv.at[p], disp_send.at[p], "sp", right)
         spread(p)
 
-    def gate_up(g, n):
-        cols = pl.ds(n * TILE, TILE)
-        rows = [
-            rows_in[j, PAIR * g : PAIR * (g + 1)].reshape(group_rows, feat) for j in range(tp_n)
-        ]
-        x = jnp.concatenate(rows, 1)
+    def gate_up(g, lo, hi):
+        cols = pl.ds(lo * TILE, (hi - lo) * TILE)
+        rows = SIZES[g] * capacity
+        x = ready[:rows]
         gate = jnp.dot(x, w_gate[:, cols], preferred_element_type=F32)
         up = jnp.dot(x, w_up[:, cols], preferred_element_type=F32)
-        hidden[g, :, cols] = (gate * jax.nn.sigmoid(gate) * up).astype(BF16)
+        hidden[g, :rows, cols] = (gate * jax.nn.sigmoid(gate) * up).astype(BF16)
 
     def down(g):
+        rows = pl.ds(0, SIZES[g] * capacity)
+
         def part(block):
-            return jnp.dot(hidden[g], w_down[:, feat_cols(block)], preferred_element_type=F32)
+            return jnp.dot(hidden[g, rows], w_down[:, feat_cols(block)], preferred_element_type=F32)
 
         for k in order:
-            part_pp[g, k] = part(2 * y_at(k) + 1 - core).astype(BF16)
+            part_pp[g, k, rows] = part(2 * y_at(k) + 1 - core).astype(BF16)
             send(
-                part_pp.at[g, k], part_a.at[g, k], part_send.at[g, k], part_recv.at[g, k],
-                "tp", partner,
+                part_pp.at[g, k, rows], part_a.at[g, k, rows],
+                part_send.at[g, k], part_recv.at[g, k], "tp", partner,
             )
-            part_own[g, k] = part(2 * y_at(k) + core)
+            part_own[g, k, rows] = part(2 * y_at(k) + core)
 
     def cross(g):
-        for k in order[:-1]:
-            arrived(part_a.at[g, k], part_recv.at[g, k], part_send.at[g, k], "tp", partner)
-            part_s[g, k] = (part_own[g, k] + part_a[g, k].astype(F32)).astype(BF16)
-            for i in ((0, 1) if g == groups - 1 else (1, 0)):
-                rows = pl.ds(i * capacity, capacity)
+        rows = pl.ds(0, SIZES[g] * capacity)
+        for k in order:
+            arrived(
+                part_a.at[g, k, rows], part_recv.at[g, k], part_send.at[g, k], "tp", partner
+            )
+            if not k:
+                continue
+            part_s[g, k, rows] = (part_own[g, k, rows] + part_a[g, k, rows].astype(F32)).astype(BF16)
+            for p in sorted(members[g], key=lambda p: -TURNS[p]):
+                i = p - begins[g]
+                one = pl.ds(i * capacity, capacity)
                 send(
-                    part_s.at[g, k, rows], part_b.at[g, k, rows],
+                    part_s.at[g, k, one], part_b.at[g, k, one],
                     cross_send.at[g, k, i], cross_recv.at[g, k, i],
                     "tp", 2 * y_at(k) + core,
                 )
-        arrived(part_a.at[g, 0], part_recv.at[g, 0], part_send.at[g, 0], "tp", partner)
 
     def finish(p):
-        g, i = p // PAIR, p % PAIR
+        g = [p in m for m in members].index(True)
+        i = p - begins[g]
         rows = pl.ds(i * capacity, capacity)
         value = part_own[g, 0, rows, :] + part_a[g, 0, rows, :].astype(F32)
         for k in range(1, y_n):
@@ -545,27 +610,27 @@
             back_in[0] = value.astype(BF16)
 
     tiles = ff // TILE
-    early = PLAN[0]
-    do = dict(D=dispatch, L=landed, F=pass_on, R=finish, X=cross)
+    do = dict(D=dispatch, S=describe, L=landed, F=pass_on, R=finish, X=cross)
 
     def act(text):
         for word in text:
             do[word[0]](int(word[1:]))
 
-    act(early)
+    act(PLAN[0])
     loads[2].wait()
     loads[3].wait()
     for g in range(groups):
-        for p in range(PAIR * g, PAIR * (g + 1)):
+        for i, p in enumerate(members[g]):
             gathered(p)
-        for n in range(tiles):
-            gate_up(g, n)
-            if n % 2 or n == tiles - 1:
-                act(PLAN[1 + g][n // 2])
+            normalize(g, i, p)
+        act(PLAN[1 + g][0])
+        for n in range(0, tiles, 2):
+            gate_up(g, n, min(n + 2, tiles))
+            act(PLAN[1 + g][1 + n // 2])
         if g == 0:
             loads[4].wait()
         down(g)
-        act(PLAN[1 + g][3])
+        act(PLAN[1 + g][4])
     act(PLAN[-1])
 
     def combine(lo, hi):
@@ -578,7 +643,7 @@
         pick1 = jnp.dot((s_lane == slot_col1).astype(F32).astype(BF16), rows, preferred_element_type=F32)
         return by_col[:, 3:4] * pick0 + by_col[:, 4:5] * pick1
 
-    moe = combine(0, sp_n - PAIR) + combine(sp_n - PAIR, sp_n)
+    moe = combine(0, begins[-1]) + combine(begins[-1], sp_n)
     pre = residual_alpha * mixed[...].astype(F32) + moe
     mean, scale = stats(2, pre, feat * tp_n)
     out[...] = ((pre - mean) * scale * final_gain[...]).astype(BF16)
@@ -613,7 +678,8 @@
     width, ff = expert_gate.shape[1:]
     capacity = 4 * tok // sp_n
     y_n = tp_n // 2
-    groups, rows = sp_n // PAIR, PAIR * capacity
+    groups, most = len(SIZES), max(SIZES)
+    rows = most * capacity
     wide = -(-tok // 128) * 128
     vmem = pl.BlockSpec(memory_space=pltpu.VMEM)
     hbm = pl.BlockSpec(memory_space=pl.ANY)
@@ -647,7 +713,12 @@
         pltpu.VMEM((y_n, tok, feat), BF16),
         pltpu.VMEM((y_n, tok, feat), BF16),
         pltpu.VMEM((y_n, tok, feat), BF16),
+        pltpu.VMEM((tok, feat), F32),
         pltpu.VMEM((tok, feat), BF16),
+        pltpu.VMEM((tok, feat), BF16),
+        pltpu.VMEM((rows, width), BF16),
+        pltpu.VMEM((sp_n, 8, 128), F32),
+        pltpu.VMEM((sp_n, 8, 128), F32),
         pltpu.VMEM((sp_n, capacity, feat), BF16),
         pltpu.VMEM((tp_n, sp_n, capacity, feat), BF16),
         pltpu.VMEM((groups, rows, ff), BF16),
@@ -667,12 +738,14 @@
         dma((2, y_n)),
         dma((sp_n,)),
         dma((sp_n,)),
+        dma((sp_n,)),
+        dma((sp_n,)),
         dma((2 * y_n - 1, sp_n)),
         dma((2 * y_n - 1, sp_n)),
         dma((groups, y_n)),
         dma((groups, y_n)),
-        dma((groups, y_n, PAIR)),
-        dma((groups, y_n, PAIR)),
+        dma((groups, y_n, most)),
+        dma((groups, y_n, most)),
         dma((sp_n,)),
         dma((sp_n,)),
     ]
@@ -713,12 +786,13 @@
         and feat % TILE == 0
         and ff % TILE == 0
         and (4 * tok // sp_n) % 32 == 0
+        and 4 * tok // sp_n <= 128
         and tok % HALO == 0
         and args[3].shape[0] <= HALO
         and tp_n % 2 == 0
         and tp_n > 2
         and sp_n == len(TURNS)
-        and -(-ff // (2 * TILE)) <= len(PLAN[1]) - 1
+        and ff <= 2 * TILE * (len(PLAN[1]) - 2)
         and args[10].shape[0] == 1
     )
     return (local_kernel if aligned else local_plain)(*args)

time: 77.9 us -> 74.8 us (0.960)
  Pallas kernels: 77.1 us -> 73.9 us
    pallas_call x1, Pallas kernels: 77.1 us -> 73.9 us  [local_kernel(): pl.pallas_call(functools.partial(block_kernel, sp_n, tp_n, capacity, conv...]
where the time goes in v3:
time: 74.8 us; the launch traced here: 74.6 us
  Pallas kernels  73.9 us (99%)
    pallas_call x1, Pallas kernels, local_kernel(): pl.pallas_call(functools.partial(block_kernel, sp_n, tp_n, capacity, conv...  73.9 us

profile of v3, /device:TPU:0, one launch (start us, length us, event | category | flops | bytes accessed | tf_op | source)
XLA Modules:
  0.0 74.6 jit_solution(134086640183228838)
XLA Ops:
  0.0 73.9 %shard_map.136 = bf16[192,512]{1,0:T(8,128)(2,1)S(1)} custom-call(bf16[192,256]{1,0:T(8,128)(2,1)} %glu_value_hbm.1, bf16[192,256]{1,0:T(8,128)(2,1)} %glu_gate_hbm.1, s32[1,192]{1,0:T(1,128)} %bitcast.10, bf16[31,256]{1,0:T(8,128)(2,1)} %conv_kernel_hbm.1, f32[1,256]{1,0:T(1,128)} %bitcast.11, bf16[256,2048]{1,0:T(8,128)(2,1)} %out_weight_hbm.1, ...), custom_call_target="tpu_custom_call" | custom-call | tf_op jit(solution)/shard_map/pallas_call | solution.py:752
  74.0 0.7 copy.16

commit v4 on v3

--- a/solution.py
+++ b/solution.py
@@ -125,9 +125,9 @@
 SIZES = (1, 2, 2, 2, 1)
 PLAN = (
     ("D0", "D1", "D2", "S0", "F0", "D3", "D4"),
-    ((), ("L2", "D6"), ("L1", "D5"), ("D7", "F2"), ("L4", "F1", "X0")),
-    ((), ("L3",), ("F4", "L6"), (), ("F3", "L5")),
-    (("X1",), (), ("F6", "L7"), ("R0",), ("F5", "R1")),
+    ((), ("L2", "D6"), ("L1", "D5"), ("D7", "F2"), ("L4", "F1", "L3", "X0")),
+    ((), ("L6",), ("F4",), ("L5",), ("F3",)),
+    (("X1",), ("L7",), ("F6",), ("R0",), ("F5", "R1")),
     (("X2",), ("R2",), (), (), ("F7", "R3")),
     (("X3",), ("R4",), (), (), ()),
     ("X4", "R5", "R6", "R7"),

time: 74.8 us -> 74.1 us (level)
  no operation moved by 1% of the time
where the time goes in v4:
time: 74.1 us; the launch traced here: 74 us
  Pallas kernels  73.3 us (99%)
    pallas_call x1, Pallas kernels, local_kernel(): pl.pallas_call(functools.partial(block_kernel, sp_n, tp_n, capacity, conv...  73.3 us

profile of v4, /device:TPU:0, one launch (start us, length us, event | category | flops | bytes accessed | tf_op | source)
XLA Modules:
  0.0 74.0 jit_solution(15836348099020335623)
XLA Ops:
  0.0 73.3 %shard_map.136 = bf16[192,512]{1,0:T(8,128)(2,1)S(1)} custom-call(bf16[192,256]{1,0:T(8,128)(2,1)} %glu_value_hbm.1, bf16[192,256]{1,0:T(8,128)(2,1)} %glu_gate_hbm.1, s32[1,192]{1,0:T(1,128)} %bitcast.10, bf16[31,256]{1,0:T(8,128)(2,1)} %conv_kernel_hbm.1, f32[1,256]{1,0:T(1,128)} %bitcast.11, bf16[256,2048]{1,0:T(8,128)(2,1)} %out_weight_hbm.1, ...), custom_call_target="tpu_custom_call" | custom-call | tf_op jit(solution)/shard_map/pallas_call | solution.py:752
  73.3 0.7 copy.16
